TPU v7x, 32 devices: a whole 2x2x4 slice. The times are simulated.
32 devices in a mesh: gr: 2 (over x), fs: 8 (over z, y), tp: 2 (over core).
Axes of the slice: x: 2, y: 2, z: 4, core: 2. Of those that a mesh axis runs over, the one named last changes fastest.
Arguments:
- prompt: bfloat16 [3072, 2048], P(('gr', 'fs', 'tp')), may hold values from -6 to 6
- norm_first: float32 [2048], P(('gr', 'fs')), may hold values from 0.1 to 1.9
- gate_first: float32 [2048, 5632], P(('gr', 'fs'), 'tp'), may hold values from -6 to 6
- up_first: float32 [2048, 5632], P(('gr', 'fs'), 'tp'), may hold values from -6 to 6
- down_first: float32 [2048, 5632], P(('gr', 'fs'), 'tp'), may hold values from -6 to 6
- norm_second: float32 [2048], P(('gr', 'fs')), may hold values from 0.1 to 1.9
- gate_second: float32 [2048, 5632], P(('gr', 'fs'), 'tp'), may hold values from -6 to 6
- up_second: float32 [2048, 5632], P(('gr', 'fs'), 'tp'), may hold values from -6 to 6
- down_second: float32 [2048, 5632], P(('gr', 'fs'), 'tp'), may hold values from -6 to 6
Outputs:
- served_gate_first: bfloat16 [2048, 5632], P(None, 'fs')
- served_up_first: bfloat16 [2048, 5632], P(None, 'fs')
- served_down_first: bfloat16 [2048, 5632], P(None, 'fs')
- served_gate_second: bfloat16 [2048, 5632], P(None, 'fs')
- served_up_second: bfloat16 [2048, 5632], P(None, 'fs')
- served_down_second: bfloat16 [2048, 5632], P(None, 'fs')
- result: bfloat16 [3072, 2048], P(('gr', 'fs', 'tp'))
All inputs are finite; a program needn't handle non-finite values.
Results may differ from a plain program's by a relative error of at most 0.015.
Values may be sent and summed in bfloat16 or wider, within the bound.
A program may use at most 128 MiB of HBM per device.

v0:
```python
import jax
import jax.numpy as jnp
from jax import lax
from jax.sharding import PartitionSpec as P

D = 2048
FF = 5632
EPS = 1e-06


def fold_rows(gain, weight):
    return (gain[:, None] * weight).astype(jnp.bfloat16)


def relayout(stacked):
    moved = lax.all_to_all(
        lax.all_to_all(stacked, "tp", split_axis=1, concat_axis=2, tiled=True),
        "fs",
        split_axis=2,
        concat_axis=1,
        tiled=True,
    )
    whole = lax.all_gather(moved, ("gr", "tp"), axis=1, tiled=True)
    matrices = stacked.shape[0]
    block_width = moved.shape[2]
    gr_size = lax.axis_size("gr")
    tp_size = lax.axis_size("tp")
    fs_size = lax.axis_size("fs")
    sub_rows = stacked.shape[1] // tp_size
    shaped = whole.reshape(matrices, gr_size, tp_size, fs_size, sub_rows, block_width)
    return shaped.transpose(0, 1, 3, 2, 4, 5).reshape(
        matrices, gr_size * fs_size * tp_size * sub_rows, block_width
    )


def half_step(residual, weights):
    gate_weight = weights[0]
    up_weight = weights[1]
    down_weight = weights[2]
    resid_f = residual.astype(jnp.float32)
    normed = (
        resid_f * lax.rsqrt(jnp.mean(resid_f * resid_f, axis=-1, keepdims=True) + EPS)
    ).astype(jnp.bfloat16)
    in_scale = D ** (-0.5)
    out_scale = FF ** (-0.5)
    tokens_in = lax.all_gather(normed, "fs", axis=0, tiled=True)
    gate_pre = jnp.dot(tokens_in, gate_weight, preferred_element_type=jnp.float32) * in_scale
    up_pre = jnp.dot(tokens_in, up_weight, preferred_element_type=jnp.float32) * in_scale
    hidden = (jax.nn.silu(gate_pre) * up_pre).astype(jnp.bfloat16)
    branch = lax.psum_scatter(
        (
            lax.dot_general(
                hidden, down_weight, (((1,), (1,)), ((), ())), preferred_element_type=jnp.float32
            )
            * out_scale
        ).astype(jnp.bfloat16),
        "fs",
        scatter_dimension=0,
        tiled=True,
    ).astype(jnp.float32)
    return (resid_f + 0.5 * branch).astype(jnp.bfloat16)


def on_device(
    prompt,
    norm_first,
    gate_first,
    up_first,
    down_first,
    norm_second,
    gate_second,
    up_second,
    down_second,
):
    first_set = jnp.stack(
        [
            fold_rows(norm_first, gate_first),
            fold_rows(norm_first, up_first),
            down_first.astype(jnp.bfloat16),
        ]
    )
    second_set = jnp.stack(
        [
            fold_rows(norm_second, gate_second),
            fold_rows(norm_second, up_second),
            down_second.astype(jnp.bfloat16),
        ]
    )
    served_first = relayout(first_set)
    middle = half_step(prompt, served_first)
    served_second = relayout(second_set)
    result = half_step(middle, served_second)
    return (
        served_first[0],
        served_first[1],
        served_first[2],
        served_second[0],
        served_second[1],
        served_second[2],
        result,
    )


def solution(mesh):
    in_specs = (
        P(("gr", "fs", "tp"), None),
        P(("gr", "fs")),
        P(("gr", "fs"), "tp"),
        P(("gr", "fs"), "tp"),
        P(("gr", "fs"), "tp"),
        P(("gr", "fs")),
        P(("gr", "fs"), "tp"),
        P(("gr", "fs"), "tp"),
        P(("gr", "fs"), "tp"),
    )
    out_specs = (
        P(None, "fs"),
        P(None, "fs"),
        P(None, "fs"),
        P(None, "fs"),
        P(None, "fs"),
        P(None, "fs"),
        P(("gr", "fs", "tp"), None),
    )
    return jax.shard_map(
        on_device, mesh=mesh, in_specs=in_specs, out_specs=out_specs, check_vma=False
    )
```

profile of v0, /device:TPU:0, one launch (start us, length us, event | category | flops | bytes accessed | tf_op | source)
XLA Modules:
  0.0 607.6 jit_solution(7273351563624397723)
XLA Ops:
  7.2 2.5 fusion.6
  11.8 6.0 all_to_all.72
  17.9 2.6 copy.77
  20.5 10.8 %copy.72 = bf16[3,64,2,2816]{1,0,3,2:T(4,128)(2,1)} copy(bf16[3,64,2,2816]{3,2,1,0:T(2,128)(2,1)S(1)} %bitcast.78) | data formatting | bytes 4325376 | tf_op jit(solution)/shard_map/all_to_all | solution.py:17
  31.3 7.1 %reshape.54 = bf16[8,2,67584]{2,1,0:T(2,128)(2,1)S(1)} reshape(bf16[5632,3,64]{2,1,0:T(4,128)(2,1)} %bitcast.56) | data formatting | bytes 4325376
  38.4 57.7 %all_to_all.73 = bf16[8,2,67584]{2,1,0:T(2,128)(2,1)} all-to-all(bf16[8,2,67584]{2,1,0:T(2,128)(2,1)S(1)} %reshape.54), channel_id=1, replica_groups=mesh['gr'=2,'fs'=8,'tp'=2] {'fs'}, dimensions={0} | all-to-all | bytes 4325376 | tf_op jit(solution)/shard_map/all_to_all | solution.py:16
  96.1 8.0 %reshape.55 = bf16[5632,3,64]{2,1,0:T(4,128)(2,1)} reshape(bf16[8,2,67584]{2,1,0:T(2,128)(2,1)} %all_to_all.73) | data formatting | bytes 4325376
  104.1 9.4 %copy.55 = bf16[3,64,8,704]{3,1,2,0:T(8,128)(2,1)} copy(bf16[3,64,8,704]{1,0,3,2:T(4,128)(2,1)} %bitcast.57) | data formatting | bytes 4325376 | tf_op jit(solution)/shard_map/all_to_all | solution.py:16
  115.0 61.3 %all-gather.5.cloned.1.call-done = bf16[3,2048,704]{2,1,0:T(8,128)(2,1)} async-done(((bf16[3,512,704]{2,1,0:T(8,128)(2,1)}), bf16[3,2048,704]{2,1,0:T(8,128)(2,1)}) %all-gather.5.cloned.1.call-update) | async-done | bytes 8650768 | tf_op jit(solution)/shard_map/all_gather | solution.py:23
  176.3 4.1 fusion.15
  184.5 54.6 %all-gather.9.cloned.1.call-done = bf16[768,2048]{1,0:T(8,128)(2,1)} async-done(((bf16[96,2048]{1,0:T(8,128)(2,1)}), bf16[768,2048]{1,0:T(8,128)(2,1)}) %all-gather.9.cloned.1.call-update) | async-done | bytes 3145744 | tf_op jit(solution)/shard_map/all_gather | solution.py:46
  239.1 5.7 fusion.16
  244.8 12.4 %multiply_convert_fusion.1 = bf16[768,2048]{1,0:T(8,128)(2,1)} fusion(bf16[2048,704]{1,0:T(8,128)(2,1)} %bitcast.64, f32[768,704]{0,1:T(8,128)} %fusion.16, bf16[768,2048]{1,0:T(8,128)(2,1)} %all-gather.9.cloned.1.call-done, bf16[2048,704]{1,0:T(8,128)(2,1)} %bitcast.62), kind=kOutput, calls=%fused_computation.1 | convolution fusion | flops 4436656128 | bytes 14221312 | tf_op jit(solution)/shard_map/dot_general | solution.py:52
  262.5 6.0 all_to_all.74
  268.5 3.9 copy.76
  272.5 15.1 %copy.73 = bf16[3,64,2,2816]{1,0,3,2:T(4,128)(2,1)} copy(bf16[3,64,2,2816]{3,2,1,0:T(2,128)(2,1)} %bitcast.79) | data formatting | bytes 4325376 | tf_op jit(solution)/shard_map/all_to_all | solution.py:17
  287.6 8.2 %reshape.56 = bf16[8,2,67584]{2,1,0:T(2,128)(2,1)} reshape(bf16[5632,3,64]{2,1,0:T(4,128)(2,1)} %bitcast.58) | data formatting | bytes 4325376
  295.9 67.8 %all_to_all.75 = bf16[8,2,67584]{2,1,0:T(2,128)(2,1)} all-to-all(bf16[8,2,67584]{2,1,0:T(2,128)(2,1)} %reshape.56), channel_id=1, replica_groups=mesh['gr'=2,'fs'=8,'tp'=2] {'fs'}, dimensions={0} | all-to-all | bytes 4325376 | tf_op jit(solution)/shard_map/all_to_all | solution.py:16
  363.7 8.0 %reshape.57 = bf16[5632,3,64]{2,1,0:T(4,128)(2,1)} reshape(bf16[8,2,67584]{2,1,0:T(2,128)(2,1)} %all_to_all.75) | data formatting | bytes 4325376
  371.6 9.4 %copy.62 = bf16[3,64,8,704]{3,1,2,0:T(8,128)(2,1)} copy(bf16[3,64,8,704]{1,0,3,2:T(4,128)(2,1)} %bitcast.59) | data formatting | bytes 4325376 | tf_op jit(solution)/shard_map/all_to_all | solution.py:16
  384.5 59.3 %all-gather.7.cloned.1.call-done = bf16[3,2048,704]{2,1,0:T(8,128)(2,1)} async-done(((bf16[3,512,704]{2,1,0:T(8,128)(2,1)}), bf16[3,2048,704]{2,1,0:T(8,128)(2,1)}) %all-gather.7.cloned.1.call-update) | async-done | bytes 8650768 | tf_op jit(solution)/shard_map/all_gather | solution.py:23
  443.8 4.1 fusion.14
  453.6 52.8 %all-gather.11.cloned.1.call-done = bf16[768,2048]{1,0:T(8,128)(2,1)} async-done(((bf16[96,2048]{1,0:T(8,128)(2,1)}), bf16[768,2048]{1,0:T(8,128)(2,1)}) %all-gather.11.cloned.1.call-update) | async-done | bytes 3145744 | tf_op jit(solution)/shard_map/all_gather | solution.py:46
  506.5 6.6 %fusion.17 = f32[768,704]{0,1:T(8,128)} fusion(bf16[768,2048]{1,0:T(8,128)(2,1)} %all-gather.11.cloned.1.call-done, bf16[2048,704]{1,0:T(8,128)(2,1)} %bitcast.66), kind=kOutput, calls=%fused_computation.39 | convolution fusion | flops 2214592512 | bytes 8192000 | tf_op jit(solution)/shard_map/dot_general | solution.py:47
  513.1 12.4 %multiply_convert_fusion = bf16[768,2048]{1,0:T(8,128)(2,1)} fusion(bf16[2048,704]{1,0:T(8,128)(2,1)} %bitcast.70, f32[768,704]{0,1:T(8,128)} %fusion.17, bf16[768,2048]{1,0:T(8,128)(2,1)} %all-gather.11.cloned.1.call-done, bf16[2048,704]{1,0:T(8,128)(2,1)} %bitcast.68), kind=kOutput, calls=%fused_computation | convolution fusion | flops 4436656128 | bytes 14221312 | tf_op jit(solution)/shard_map/dot_general | solution.py:52
  525.6 4.6 copy.69
  530.1 4.6 copy.70
  534.7 4.6 copy.71
  539.2 2.7 copy.66
  541.9 4.7 copy.67
  546.7 2.7 copy.68
  549.3 49.1 %reduce-scatter.5.cloned.1.call-done = bf16[96,2048]{1,0:T(8,128)(2,1)} async-done(((bf16[768,2048]{1,0:T(8,128)(2,1)}), bf16[96,2048]{1,0:T(8,128)(2,1)}) %reduce-scatter.5.cloned.1.call-update) | async-done | bytes 393232 | tf_op jit(solution)/shard_map/reduce_scatter | solution.py:50
  (37 shorter events, 24.1 us)
Async XLA Ops:
  7.2 169.1 %all-gather.5.cloned.1.call-start = ((), (), s32[]{:S(2)}) async-start(), calls=%async_computation.6 | async-start | bytes 11796480 | tf_op jit(solution)/shard_map/all_gather | solution.py:23
  104.1 9.5 %copy-start.1 = (bf16[96,2048]{1,0:T(8,128)(2,1)S(1)}, bf16[96,2048]{1,0:T(8,128)(2,1)}, u32[]{:S(2)}) copy-start(bf16[96,2048]{1,0:T(8,128)(2,1)} %param.9) | copy-start | bytes 1179652
  113.5 125.6 %all-gather.9.cloned.1.call-start = ((), (), s32[]{:S(2)}) async-start(), calls=%async_computation.8 | async-start | bytes 3538944 | tf_op jit(solution)/shard_map/all_gather | solution.py:46
  114.7 266.4 %reduce-scatter.3.cloned.1.call-start = ((), (), s32[]{:S(2)}) async-start(), calls=%async_computation.9 | async-start | bytes 3538944 | tf_op jit(solution)/shard_map/reduce_scatter | solution.py:50
  257.2 0.7 copy-start.2
  257.3 186.5 %all-gather.7.cloned.1.call-start = ((), (), s32[]{:S(2)}) async-start(), calls=%async_computation.7 | async-start | bytes 11796480 | tf_op jit(solution)/shard_map/all_gather | solution.py:23
  381.0 125.4 %all-gather.11.cloned.1.call-start = ((), (), s32[]{:S(2)}) async-start(), calls=%async_computation.10 | async-start | bytes 3538944 | tf_op jit(solution)/shard_map/all_gather | solution.py:46
  384.3 214.2 %reduce-scatter.5.cloned.1.call-start = ((), (), s32[]{:S(2)}) async-start(), calls=%async_computation.11 | async-start | bytes 3538944 | tf_op jit(solution)/shard_map/reduce_scatter | solution.py:50
  541.9 4.7 copy-start
Sparse Core Ops, SparseCore 0:
  113.6 62.6 all-gather.4
  179.1 60.0 all-gather.8
  257.4 96.6 reduce-scatter.2
  381.2 62.5 all-gather.6
  446.4 60.0 all-gather.10
  525.7 72.7 reduce-scatter.4
where the time goes:
time: 615 us; the launch traced here: 608 us
  waiting for transfers between devices  277 us (45%)
  blocking collectives  138 us (22%)
  local copies, waits for them, and re-layouts  128 us (21%)
  matrix products  37.2 us (6%)
  between operations  14.4 us (2%)
  other arithmetic  11.8 us (2%)
    all_to_all x2, blocking collectives, relayout(): lax.all_to_all(lax.all_to_all(stacked, 'tp', split_axis=1, concat_axis=2,...  126 us
    all_gather x2, waiting for transfers between devices, relayout(): whole = lax.all_gather(moved, ('gr', 'tp'), axis=1, tiled=True)  121 us
    all_gather x2, waiting for transfers between devices, half_step(): tokens_in = lax.all_gather(normed, 'fs', axis=0, tiled=True)  107 us
    unnamed x16, local copies, waits for them, and re-layouts  55.2 us
    reduce_scatter x2, waiting for transfers between devices, half_step(): lax.psum_scatter((lax.dot_general(hidden, down_weight, (((1,), (1,)), (()...  49.1 us
    all_to_all x4, local copies, waits for them, and re-layouts, relayout(): lax.all_to_all(stacked, 'tp', split_axis=1, concat_axis=2, tiled=True)  32.4 us
    dot_general x2, matrix products, half_step(): lax.dot_general(hidden, down_weight, (((1,), (1,)), ((), ())), preferred_...  24.9 us
    all_to_all x2, local copies, waits for them, and re-layouts, relayout(): lax.all_to_all(lax.all_to_all(stacked, 'tp', split_axis=1, concat_axis=2,...  18.8 us
  transfers between devices with their start and end apart: 6, of which 5 were waited for; matrix products, arithmetic and copies ran while one was open for 16% of the time, Pallas kernels for 0%

commit v1 on v0

--- a/solution.py
+++ b/solution.py
@@ -6,6 +6,15 @@
 D = 2048
 FF = 5632
 EPS = 1e-06
+deliver_modes = lambda xin: jnp.concatenate(
+    lax.all_to_all(
+        jnp.stack(jnp.split(xin, lax.axis_size("fs"), axis=2)),
+        split_axis=0,
+        concat_axis=0,
+        axis_name="fs",
+    ),
+    axis=1,
+)
 
 
 def fold_rows(gain, weight):
@@ -13,13 +22,7 @@
 
 
 def relayout(stacked):
-    moved = lax.all_to_all(
-        lax.all_to_all(stacked, "tp", split_axis=1, concat_axis=2, tiled=True),
-        "fs",
-        split_axis=2,
-        concat_axis=1,
-        tiled=True,
-    )
+    moved = deliver_modes(lax.all_to_all(stacked, "tp", split_axis=1, concat_axis=2, tiled=True))
     whole = lax.all_gather(moved, ("gr", "tp"), axis=1, tiled=True)
     matrices = stacked.shape[0]
     block_width = moved.shape[2]

time: 615 us -> 561 us (0.912); the launches traced: 608 us -> 560 us
  local copies, waits for them, and re-layouts: 128 us -> 70.8 us
  blocking collectives: 138 us -> 147 us
    unnamed x16 -> x28, local copies, waits for them, and re-layouts: 55.2 us -> 30.2 us
    all_to_all x2 -> x0, local copies, waits for them, and re-layouts: 18.8 us -> none  [relayout(): lax.all_to_all(lax.all_to_all(stacked, 'tp', split_axis=1, concat_axis=2,...]
    all_to_all x4, local copies, waits for them, and re-layouts: 32.4 us -> 15.5 us  [relayout(): lax.all_to_all(stacked, 'tp', split_axis=1, concat_axis=2, tiled=True)]
    all_to_all x2, blocking collectives: 126 us -> 135 us  [lax.all_to_all(jnp.stack(jnp.split(xin, lax.axis_size('fs'), axis=2)), sp...]
  transfers between devices with their start and end apart: 6 -> 6, of which waited for: 5 -> 5; matrix products, arithmetic and copies ran while one was open for 16% -> 11% of each run, Pallas kernels for 0% -> 0%
where the time goes in v1:
time: 561 us; the launch traced here: 560 us
  waiting for transfers between devices  278 us (50%)
  blocking collectives  147 us (26%)
  local copies, waits for them, and re-layouts  70.8 us (13%)
  matrix products  37.2 us (7%)
  between operations  14.3 us (3%)
  other arithmetic  11.8 us (2%)
    all_to_all x2, blocking collectives, lax.all_to_all(jnp.stack(jnp.split(xin, lax.axis_size('fs'), axis=2)), sp...  135 us
    all_gather x2, waiting for transfers between devices, relayout(): whole = lax.all_gather(moved, ('gr', 'tp'), axis=1, tiled=True)  121 us
    all_gather x2, waiting for transfers between devices, half_step(): tokens_in = lax.all_gather(normed, 'fs', axis=0, tiled=True)  108 us
    reduce_scatter x2, waiting for transfers between devices, half_step(): lax.psum_scatter((lax.dot_general(hidden, down_weight, (((1,), (1,)), (()...  49.3 us
    unnamed x28, local copies, waits for them, and re-layouts  30.2 us
    dot_general x2, matrix products, half_step(): lax.dot_general(hidden, down_weight, (((1,), (1,)), ((), ())), preferred_...  24.9 us
    all_to_all x4, local copies, waits for them, and re-layouts, relayout(): lax.all_to_all(stacked, 'tp', split_axis=1, concat_axis=2, tiled=True)  15.5 us
    dot_general x2, matrix products, half_step(): jnp.dot(tokens_in, gate_weight, preferred_element_type=jnp.float32)  12.3 us
  transfers between devices with their start and end apart: 6, of which 5 were waited for; matrix products, arithmetic and copies ran while one was open for 11% of the time, Pallas kernels for 0%

profile of v1, /device:TPU:0, one launch (start us, length us, event | category | flops | bytes accessed | tf_op | source)
XLA Modules:
  0.0 559.7 jit_solution(983472712786277361)
XLA Ops:
  7.2 2.5 fusion.6
  11.8 6.0 %all_to_all.46 = bf16[3,128,2816]{2,0,1:T(4,128)(2,1)S(1)} all-to-all(bf16[3,128,2816]{2,0,1:T(4,128)(2,1)S(1)} %copy.50), channel_id=1, replica_groups=mesh['gr'=2,'fs'=8,'tp'=2] {'tp'}, dimensions={1} | all-to-all | bytes 4325376 | tf_op jit(solution)/shard_map/all_to_all | solution.py:25
  17.9 3.9 copy.71
  21.8 3.2 all_to_all.35
  25.8 61.2 %all_to_all.47 = bf16[8,3,64,704]{3,2,1,0:T(8,128)(2,1)S(1)} all-to-all(bf16[8,3,64,704]{3,2,1,0:T(8,128)(2,1)S(1)} %fusion.18), channel_id=1, replica_groups=mesh['gr'=2,'fs'=8,'tp'=2] {'fs'}, dimensions={0} | all-to-all | bytes 4325376 | tf_op jit(solution)/shard_map/all_to_all | solution.py:10
  90.9 61.1 %all-gather.5.cloned.1.call-done = bf16[3,2048,704]{2,1,0:T(8,128)(2,1)} async-done(((bf16[3,512,704]{2,1,0:T(8,128)(2,1)}), bf16[3,2048,704]{2,1,0:T(8,128)(2,1)}) %all-gather.5.cloned.1.call-update) | async-done | bytes 8650768 | tf_op jit(solution)/shard_map/all_gather | solution.py:26
  152.1 4.1 fusion.31
  160.1 54.8 %all-gather.9.cloned.1.call-done = bf16[768,2048]{1,0:T(8,128)(2,1)} async-done(((bf16[96,2048]{1,0:T(8,128)(2,1)}), bf16[768,2048]{1,0:T(8,128)(2,1)}) %all-gather.9.cloned.1.call-update) | async-done | bytes 3145744 | tf_op jit(solution)/shard_map/all_gather | solution.py:49
  214.9 5.7 %fusion.32 = f32[768,704]{0,1:T(8,128)} fusion(bf16[768,2048]{1,0:T(8,128)(2,1)} %all-gather.9.cloned.1.call-done, bf16[2048,704]{1,0:T(8,128)(2,1)S(1)} %bitcast.110), kind=kOutput, calls=%fused_computation.70 | convolution fusion | flops 2214592512 | bytes 8192000 | tf_op jit(solution)/shard_map/dot_general | solution.py:50
  220.6 12.5 %multiply_convert_fusion.1 = bf16[768,2048]{1,0:T(8,128)(2,1)} fusion(bf16[2048,704]{1,0:T(8,128)(2,1)} %bitcast.114, f32[768,704]{0,1:T(8,128)} %fusion.32, bf16[768,2048]{1,0:T(8,128)(2,1)} %all-gather.9.cloned.1.call-done, bf16[2048,704]{1,0:T(8,128)(2,1)} %bitcast.112), kind=kOutput, calls=%fused_computation.1 | convolution fusion | flops 4436656128 | bytes 14221312 | tf_op jit(solution)/shard_map/dot_general | solution.py:55
  233.7 2.5 fusion.8
  238.3 6.0 %all_to_all.48 = bf16[3,128,2816]{2,0,1:T(4,128)(2,1)S(1)} all-to-all(bf16[3,128,2816]{2,0,1:T(4,128)(2,1)S(1)} %copy.56), channel_id=1, replica_groups=mesh['gr'=2,'fs'=8,'tp'=2] {'tp'}, dimensions={1} | all-to-all | bytes 4325376 | tf_op jit(solution)/shard_map/all_to_all | solution.py:25
  244.3 3.9 copy.70
  248.3 4.4 all_to_all.40
  257.5 73.3 %all_to_all.49 = bf16[8,3,64,704]{3,2,1,0:T(8,128)(2,1)S(1)} all-to-all(bf16[8,3,64,704]{3,2,1,0:T(8,128)(2,1)S(1)} %fusion.10), channel_id=1, replica_groups=mesh['gr'=2,'fs'=8,'tp'=2] {'fs'}, dimensions={0} | all-to-all | bytes 4325376 | tf_op jit(solution)/shard_map/all_to_all | solution.py:10
  333.8 1.9 fusion.4
  336.0 60.0 %all-gather.7.cloned.1.call-done = bf16[3,2048,704]{2,1,0:T(8,128)(2,1)} async-done(((bf16[3,512,704]{2,1,0:T(8,128)(2,1)}), bf16[3,2048,704]{2,1,0:T(8,128)(2,1)}) %all-gather.7.cloned.1.call-update) | async-done | bytes 8650768 | tf_op jit(solution)/shard_map/all_gather | solution.py:26
  396.0 4.1 fusion.30
  400.1 1.9 copy.59
  402.0 1.9 copy.60
  403.9 1.9 copy.61
  405.8 52.8 %all-gather.11.cloned.1.call-done = bf16[768,2048]{1,0:T(8,128)(2,1)} async-done(((bf16[96,2048]{1,0:T(8,128)(2,1)}), bf16[768,2048]{1,0:T(8,128)(2,1)}) %all-gather.11.cloned.1.call-update) | async-done | bytes 3145744 | tf_op jit(solution)/shard_map/all_gather | solution.py:49
  458.7 6.6 %fusion.33 = f32[768,704]{0,1:T(8,128)} fusion(bf16[768,2048]{1,0:T(8,128)(2,1)} %all-gather.11.cloned.1.call-done, bf16[2048,704]{1,0:T(8,128)(2,1)} %bitcast.116), kind=kOutput, calls=%fused_computation.71 | convolution fusion | flops 2214592512 | bytes 8192000 | tf_op jit(solution)/shard_map/dot_general | solution.py:50
  465.3 12.4 %multiply_convert_fusion = bf16[768,2048]{1,0:T(8,128)(2,1)} fusion(bf16[2048,704]{1,0:T(8,128)(2,1)} %bitcast.120, f32[768,704]{0,1:T(8,128)} %fusion.33, bf16[768,2048]{1,0:T(8,128)(2,1)} %all-gather.11.cloned.1.call-done, bf16[2048,704]{1,0:T(8,128)(2,1)} %bitcast.118), kind=kOutput, calls=%fused_computation | convolution fusion | flops 4436656128 | bytes 14221312 | tf_op jit(solution)/shard_map/dot_general | solution.py:55
  477.7 4.6 copy.65
  482.3 4.6 copy.66
  486.9 4.6 copy.67
  491.4 2.7 copy.62
  494.1 4.7 copy.63
  498.9 2.7 copy.64
  501.5 49.3 %reduce-scatter.5.cloned.1.call-done = bf16[96,2048]{1,0:T(8,128)(2,1)} async-done(((bf16[768,2048]{1,0:T(8,128)(2,1)}), bf16[96,2048]{1,0:T(8,128)(2,1)}) %reduce-scatter.5.cloned.1.call-update) | async-done | bytes 393232 | tf_op jit(solution)/shard_map/reduce_scatter | solution.py:53
  550.8 2.1 fusion.5
  (51 shorter events, 21.4 us)
Async XLA Ops:
  7.2 144.9 %all-gather.5.cloned.1.call-start = ((), (), s32[]{:S(2)}) async-start(), calls=%async_computation.6 | async-start | bytes 11796480 | tf_op jit(solution)/shard_map/all_gather | solution.py:26
  88.6 1.0 copy-start.1
  88.6 126.2 %all-gather.9.cloned.1.call-start = ((), (), s32[]{:S(2)}) async-start(), calls=%async_computation.8 | async-start | bytes 3538944 | tf_op jit(solution)/shard_map/all_gather | solution.py:49
  90.7 241.8 %reduce-scatter.3.cloned.1.call-start = ((), (), s32[]{:S(2)}) async-start(), calls=%async_computation.9 | async-start | bytes 3538944 | tf_op jit(solution)/shard_map/reduce_scatter | solution.py:53
  233.0 0.7 copy-start.3
  233.1 162.9 %all-gather.7.cloned.1.call-start = ((), (), s32[]{:S(2)}) async-start(), calls=%async_computation.7 | async-start | bytes 11796480 | tf_op jit(solution)/shard_map/all_gather | solution.py:26
  252.7 4.4 copy-start.2
  332.5 126.2 %all-gather.11.cloned.1.call-start = ((), (), s32[]{:S(2)}) async-start(), calls=%async_computation.10 | async-start | bytes 3538944 | tf_op jit(solution)/shard_map/all_gather | solution.py:49
  335.7 215.1 %reduce-scatter.5.cloned.1.call-start = ((), (), s32[]{:S(2)}) async-start(), calls=%async_computation.11 | async-start | bytes 3538944 | tf_op jit(solution)/shard_map/reduce_scatter | solution.py:53
  494.1 4.7 copy-start
Sparse Core Ops, SparseCore 0:
  88.8 63.2 all-gather.4
  154.8 60.0 all-gather.8
  233.2 92.8 reduce-scatter.2
  332.6 63.3 all-gather.6
  398.6 60.0 all-gather.10
  477.9 72.9 reduce-scatter.4
